TPU v7x, 32 devices: a whole 2x2x4 slice. The times are simulated.
32 devices in a mesh: sp: 8 (over z, y), tp: 4 (over x, core).
Axes of the slice: x: 2, y: 2, z: 4, core: 2. Of those that a mesh axis runs over, the one named last changes fastest.
Arguments:
- stream: bfloat16 [2048, 2048], P('sp', 'tp'), may hold values from -6 to 6
- norm_gain: float32 [2, 2048], replicated, may hold values from 0.1 to 1.9
- w_value: bfloat16 [2, 2048, 1024], P(None, 'sp', 'tp'), may hold values from -0.125 to 0.125
- w_gate: bfloat16 [2, 2048, 1024], P(None, 'sp', 'tp'), may hold values from -0.125 to 0.125
- conv_taps: float32 [2, 128, 1024], P(None, None, 'tp'), as said below
- channel_gain: float32 [2, 1024], P(None, 'tp'), may hold values from 0.1 to 1.9
- w_out: bfloat16 [2, 1024, 2048], P(None, 'tp', 'sp'), may hold values from -0.1875 to 0.1875
Outputs:
- result: bfloat16 [2048, 2048], P('sp', 'tp')
Inputs may be any that keep to these rules, and one draw needn't show every extreme that they name: `conv_taps`: taps of each block of 128 consecutive channels share a scale factor of its own.
All inputs are finite; a program needn't handle non-finite values.
Results may differ from a plain program's by a relative error of at most 0.012.
Values may be sent and summed in bfloat16 or wider, within the bound.
A program may use at most 64 MiB of HBM per device.

v0:
```python
import jax
import jax.numpy as jnp
from jax import lax
from jax.sharding import PartitionSpec as P

C = 1024
LAYERS = 2


def from_behind(value, axis, steps):
    count = lax.axis_size(axis)
    initial, last = (max(0, -steps), min(count, count - steps))
    return lax.ppermute(value, axis, [(source, source + steps) for source in range(initial, last)])


def shards(stream, norm_gain, w_value, w_gate, conv_taps, channel_gain, w_out):
    x = stream
    tokens_here = stream.shape[0]
    local_ch = w_value.shape[2]
    taps = conv_taps.shape[1]
    for layer in range(LAYERS):
        whole = lax.all_gather(x, "tp", axis=1, tiled=True).astype(jnp.float32)
        normed = (
            whole
            * lax.rsqrt(jnp.mean(whole * whole, axis=1, keepdims=True) + 1e-06)
            * norm_gain[layer]
        ).astype(jnp.bfloat16)
        value_whole, gate_whole = (
            lax.all_gather(w_value[layer], "sp", axis=0, tiled=True),
            lax.all_gather(w_gate[layer], "sp", axis=0, tiled=True),
        )
        value = jnp.dot(normed, value_whole, preferred_element_type=jnp.float32)
        gate = jnp.dot(normed, gate_whole, preferred_element_type=jnp.float32)
        glu = (value * jax.nn.sigmoid(gate)).astype(jnp.bfloat16)
        before = from_behind(glu[tokens_here - taps :], "sp", 1)
        padded = jnp.concatenate([before[1:], glu], axis=0).astype(jnp.float32)
        conv = lax.conv_general_dilated(
            padded[None],
            conv_taps[layer][:, None, :],
            (1,),
            "VALID",
            dimension_numbers=("NWC", "WIO", "NWC"),
            feature_group_count=local_ch,
            precision=lax.Precision.HIGHEST,
        )[0]
        mean = lax.psum(jnp.sum(conv, axis=1, keepdims=True), "tp") / C
        centred = conv - mean
        spread = lax.psum(jnp.sum(centred * centred, axis=1, keepdims=True), "tp") / C
        act = jax.nn.silu(centred * lax.rsqrt(spread + 1e-05) * channel_gain[layer]).astype(
            jnp.bfloat16
        )
        out_whole = lax.all_gather(w_out[layer], "sp", axis=1, tiled=True)
        terms = jnp.dot(act, out_whole, preferred_element_type=jnp.float32)
        branch = lax.psum_scatter(terms, "tp", scatter_dimension=1, tiled=True)
        x = (x.astype(jnp.float32) + branch).astype(jnp.bfloat16)
    return x


def solution(mesh):
    return jax.shard_map(
        shards,
        mesh=mesh,
        in_specs=(
            P("sp", "tp"),
            P(),
            P(None, "sp", "tp"),
            P(None, "sp", "tp"),
            P(None, None, "tp"),
            P(None, "tp"),
            P(None, "tp", "sp"),
        ),
        out_specs=P("sp", "tp"),
        check_vma=False,
    )
```

profile of v0, /device:TPU:0, one launch (start us, length us, event | category | flops | bytes accessed | tf_op | source)
XLA Modules:
  0.0 370.0 jit_solution(6867189528916284857)
XLA Ops:
  7.3 1.7 fusion.46
  9.1 1.7 fusion.45
  10.8 1.7 fusion.47
  12.7 15.7 %all-gather.15.cloned.1.call-done = bf16[256,2048]{1,0:T(8,128)(2,1)} async-done(((bf16[256,512]{1,0:T(8,128)(2,1)}), bf16[256,2048]{1,0:T(8,128)(2,1)}) %all-gather.15.cloned.1.call-update) | async-done | bytes 1048592 | tf_op jit(solution)/shard_map/all_gather | solution.py:22
  30.0 40.8 %all-gather.19.cloned.1.call-done = bf16[1,2048,256]{2,1,0:T(8,128)(2,1)} async-done(((bf16[1,256,256]{2,1,0:T(8,128)(2,1)}), bf16[1,2048,256]{2,1,0:T(8,128)(2,1)}) %all-gather.19.cloned.1.call-update) | async-done | bytes 1048592 | tf_op jit(solution)/shard_map/all_gather | solution.py:29
  70.8 2.0 fusion.24
  72.8 39.1 %all-gather.21.cloned.1.call-done = bf16[1,2048,256]{2,1,0:T(8,128)(2,1)} async-done(((bf16[1,256,256]{2,1,0:T(8,128)(2,1)}), bf16[1,2048,256]{2,1,0:T(8,128)(2,1)}) %all-gather.21.cloned.1.call-update) | async-done | bytes 1048592 | tf_op jit(solution)/shard_map/all_gather | solution.py:30
  111.9 1.7 fusion.14
  113.7 2.5 collective-permute-start
  116.2 1.9 collective-permute-done
  118.1 4.8 %fusion.50 = (f32[256]{0:T(256)S(1)}, f32[1,256,256]{2,0,1:T(1,128)S(1)}) fusion(f32[1,128,256]{2,1,0:T(8,128)S(1)} %get-tuple-element.6, bf16[1,383,256]{2,1,0:T(8,128)(2,1)S(1)} %maximum_bitcast_fusion), kind=kOutput, calls=%fused_computation.70 | convolution fusion | flops 100728576 | bytes 590336 | tf_op jit(solution)/shard_map/conv_general_dilated | solution.py:37
  123.0 5.7 %psum.28 = f32[256,1]{0,1:T(1,128)S(1)} all-reduce(f32[256,1]{0,1:T(1,128)S(1)} %bitcast.72), channel_id=1, replica_groups=mesh['sp'=8,'tp'=4] {'tp'}, use_global_device_ids=true, to_apply=%region_2.0 | all-reduce | flops 256 | bytes 2048 | tf_op jit(solution)/shard_map/psum | solution.py:46
  128.8 7.0 %psum.29 = f32[256,1]{0,1:T(1,128)S(1)} all-reduce(f32[256,1]{0,1:T(1,128)S(1)} %bitcast.68), channel_id=1, replica_groups=mesh['sp'=8,'tp'=4] {'tp'}, use_global_device_ids=true, to_apply=%region_4.0 | all-reduce | flops 256 | bytes 2048 | tf_op jit(solution)/shard_map/psum | solution.py:48
  135.8 16.2 %all-gather.23.cloned.1.call-done = bf16[1,256,2048]{2,1,0:T(8,128)(2,1)} async-done(((bf16[1,256,256]{2,1,0:T(8,128)(2,1)}), bf16[1,256,2048]{2,1,0:T(8,128)(2,1)}) %all-gather.23.cloned.1.call-update) | async-done | bytes 1048592 | tf_op jit(solution)/shard_map/all_gather | solution.py:52
  152.0 3.1 fusion.21
  155.2 30.3 %reduce-scatter.3.cloned.1.call-done = f32[256,512]{1,0:T(8,128)} async-done(((f32[256,2048]{1,0:T(8,128)}), f32[256,512]{1,0:T(8,128)}) %reduce-scatter.3.cloned.1.call-update) | async-done | bytes 524304 | tf_op jit(solution)/shard_map/reduce_scatter | solution.py:54
  185.4 1.8 add_convert_fusion.1
  189.6 14.6 %all-gather.17.cloned.1.call-done = bf16[256,2048]{1,0:T(8,128)(2,1)} async-done(((bf16[256,512]{1,0:T(8,128)(2,1)}), bf16[256,2048]{1,0:T(8,128)(2,1)}) %all-gather.17.cloned.1.call-update) | async-done | bytes 1048592 | tf_op jit(solution)/shard_map/all_gather | solution.py:22
  204.1 1.6 fusion.3
  205.8 40.8 %all-gather.25.cloned.1.call-done = bf16[1,2048,256]{2,1,0:T(8,128)(2,1)} async-done(((bf16[1,256,256]{2,1,0:T(8,128)(2,1)}), bf16[1,2048,256]{2,1,0:T(8,128)(2,1)}) %all-gather.25.cloned.1.call-update) | async-done | bytes 1048592 | tf_op jit(solution)/shard_map/all_gather | solution.py:29
  246.6 2.0 fusion.19
  248.6 39.1 %all-gather.27.cloned.1.call-done = bf16[1,2048,256]{2,1,0:T(8,128)(2,1)} async-done(((bf16[1,256,256]{2,1,0:T(8,128)(2,1)}), bf16[1,2048,256]{2,1,0:T(8,128)(2,1)}) %all-gather.27.cloned.1.call-update) | async-done | bytes 1048592 | tf_op jit(solution)/shard_map/all_gather | solution.py:30
  287.7 1.7 fusion.15
  289.5 2.5 collective-permute-start.1
  292.0 1.9 collective-permute-done.1
  293.9 4.8 %fusion.51 = (f32[256]{0:T(256)S(1)}, f32[1,256,256]{2,0,1:T(1,128)S(1)}) fusion(f32[1,128,256]{2,1,0:T(8,128)S(1)} %get-tuple-element.5, bf16[1,383,256]{2,1,0:T(8,128)(2,1)S(1)} %maximum_bitcast_fusion.1), kind=kOutput, calls=%fused_computation.71 | convolution fusion | flops 100728576 | bytes 590336 | tf_op jit(solution)/shard_map/conv_general_dilated | solution.py:37
  298.8 5.7 %psum.30 = f32[256,1]{0,1:T(1,128)S(1)} all-reduce(f32[256,1]{0,1:T(1,128)S(1)} %bitcast.73), channel_id=1, replica_groups=mesh['sp'=8,'tp'=4] {'tp'}, use_global_device_ids=true, to_apply=%region_8.9 | all-reduce | flops 256 | bytes 2048 | tf_op jit(solution)/shard_map/psum | solution.py:46
  304.6 7.0 %psum.31 = f32[256,1]{0,1:T(1,128)S(1)} all-reduce(f32[256,1]{0,1:T(1,128)S(1)} %bitcast.69), channel_id=1, replica_groups=mesh['sp'=8,'tp'=4] {'tp'}, use_global_device_ids=true, to_apply=%region_10.11 | all-reduce | flops 256 | bytes 2048 | tf_op jit(solution)/shard_map/psum | solution.py:48
  311.6 16.3 %all-gather.29.cloned.1.call-done = bf16[1,256,2048]{2,1,0:T(8,128)(2,1)} async-done(((bf16[1,256,256]{2,1,0:T(8,128)(2,1)}), bf16[1,256,2048]{2,1,0:T(8,128)(2,1)}) %all-gather.29.cloned.1.call-update) | async-done | bytes 1048592 | tf_op jit(solution)/shard_map/all_gather | solution.py:52
  327.9 3.1 fusion.16
  331.1 30.3 %reduce-scatter.5.cloned.1.call-done = f32[256,512]{1,0:T(8,128)} async-done(((f32[256,2048]{1,0:T(8,128)}), f32[256,512]{1,0:T(8,128)}) %reduce-scatter.5.cloned.1.call-update) | async-done | bytes 524304 | tf_op jit(solution)/shard_map/reduce_scatter | solution.py:54
  361.4 1.8 add_convert_fusion
  (52 shorter events, 5.5 us)
Async XLA Ops:
  6.5 6.1 %copy-start.5 = (f32[2,2048]{1,0:T(2,128)S(1)}, f32[2,2048]{1,0:T(2,128)}, u32[]{:S(2)}) copy-start(f32[2,2048]{1,0:T(2,128)} %param.8) | copy-start | bytes 49156
  6.5 6.1 %copy-start.4 = (f32[2,128,256]{2,1,0:T(8,128)S(1)}, f32[2,128,256]{2,1,0:T(8,128)}, u32[]{:S(2)}) copy-start(f32[2,128,256]{2,1,0:T(8,128)} %param.11) | copy-start | bytes 786436
  6.5 21.8 %all-gather.15.cloned.1.call-start = ((), (), s32[]{:S(2)}) async-start(), calls=%async_computation.2 | async-start | bytes 1310720 | tf_op jit(solution)/shard_map/all_gather | solution.py:22
  7.3 63.5 %all-gather.19.cloned.1.call-start = ((), (), s32[]{:S(2)}) async-start(), calls=%async_computation.6 | async-start | bytes 1179648 | tf_op jit(solution)/shard_map/all_gather | solution.py:29
  9.0 102.9 %all-gather.21.cloned.1.call-start = ((), (), s32[]{:S(2)}) async-start(), calls=%async_computation.7 | async-start | bytes 1179648 | tf_op jit(solution)/shard_map/all_gather | solution.py:30
  10.8 141.2 %all-gather.23.cloned.1.call-start = ((), (), s32[]{:S(2)}) async-start(), calls=%async_computation.8 | async-start | bytes 1179648 | tf_op jit(solution)/shard_map/all_gather | solution.py:52
  12.6 172.9 %reduce-scatter.3.cloned.1.call-start = ((), (), s32[]{:S(2)}) async-start(), calls=%async_computation.3 | async-start | bytes 2621440 | tf_op jit(solution)/shard_map/reduce_scatter | solution.py:54
  28.4 83.6 %copy-start.1 = (bf16[256,2048]{1,0:T(8,128)(2,1)S(1)}, bf16[256,2048]{1,0:T(8,128)(2,1)}, u32[]{:S(2)}) copy-start(bf16[256,2048]{1,0:T(8,128)(2,1)} %all-gather.15.cloned.1.call-done) | copy-start | bytes 3145732
  72.8 43.4 %copy-start.6 = (f32[2,256]{1,0:T(2,128)S(1)}, f32[2,256]{1,0:T(2,128)}, u32[]{:S(2)}) copy-start(f32[2,256]{1,0:T(2,128)} %param.12) | copy-start | bytes 6148
  113.7 4.4 %collective-permute-start = (bf16[128,256]{1,0:T(8,128)(2,1)S(1)}, bf16[128,256]{1,0:T(8,128)(2,1)S(1)}, u32[]{:S(2)}, u32[]{:S(2)}) collective-permute-start(bf16[128,256]{1,0:T(8,128)(2,1)S(1)} %slice.64), channel_id=1, source_target_pairs={{0,4},{4,8},{8,12},{12,16},{16,20},{20,24},{24,28},{1,5},{5,9},{9,... | collective-permute-start | bytes 196616 | tf_op jit(solution)/shard_map/ppermute | solution.py:13
  152.0 33.5 %copy-start.3 = (bf16[256,512]{1,0:T(8,128)(2,1)S(1)}, bf16[256,512]{1,0:T(8,128)(2,1)}, u32[]{:S(2)}) copy-start(bf16[256,512]{1,0:T(8,128)(2,1)} %param.7) | copy-start | bytes 786436
  155.1 49.0 %all-gather.17.cloned.1.call-start = ((), (), s32[]{:S(2)}) async-start(), calls=%async_computation.4 | async-start | bytes 1310720 | tf_op jit(solution)/shard_map/all_gather | solution.py:22
  187.3 59.3 %all-gather.25.cloned.1.call-start = ((), (), s32[]{:S(2)}) async-start(), calls=%async_computation.9 | async-start | bytes 1179648 | tf_op jit(solution)/shard_map/all_gather | solution.py:29
  188.0 99.7 %all-gather.27.cloned.1.call-start = ((), (), s32[]{:S(2)}) async-start(), calls=%async_computation.10 | async-start | bytes 1179648 | tf_op jit(solution)/shard_map/all_gather | solution.py:30
  188.8 139.1 %all-gather.29.cloned.1.call-start = ((), (), s32[]{:S(2)}) async-start(), calls=%async_computation.11 | async-start | bytes 1179648 | tf_op jit(solution)/shard_map/all_gather | solution.py:52
  189.5 171.9 %reduce-scatter.5.cloned.1.call-start = ((), (), s32[]{:S(2)}) async-start(), calls=%async_computation.5 | async-start | bytes 2621440 | tf_op jit(solution)/shard_map/reduce_scatter | solution.py:54
  204.1 83.6 %copy-start.2 = (bf16[256,2048]{1,0:T(8,128)(2,1)S(1)}, bf16[256,2048]{1,0:T(8,128)(2,1)}, u32[]{:S(2)}) copy-start(bf16[256,2048]{1,0:T(8,128)(2,1)} %all-gather.17.cloned.1.call-done) | copy-start | bytes 3145732
  289.5 4.4 %collective-permute-start.1 = (bf16[128,256]{1,0:T(8,128)(2,1)S(1)}, bf16[128,256]{1,0:T(8,128)(2,1)S(1)}, u32[]{:S(2)}, u32[]{:S(2)}) collective-permute-start(bf16[128,256]{1,0:T(8,128)(2,1)S(1)} %slice.66), channel_id=1, source_target_pairs={{0,4},{4,8},{8,12},{12,16},{16,20},{20,24},{24,28},{1,5},{5,9},{9,... | collective-permute-start | bytes 196616 | tf_op jit(solution)/shard_map/ppermute | solution.py:13
  327.9 33.5 %copy-start = (bf16[256,512]{1,0:T(8,128)(2,1)S(1)}, bf16[256,512]{1,0:T(8,128)(2,1)}, u32[]{:S(2)}) copy-start(bf16[256,512]{1,0:T(8,128)(2,1)} %add_convert_fusion.1) | copy-start | bytes 786436
Sparse Core Ops, SparseCore 0:
  8.9 19.4 all-gather.14
  30.5 40.2 all-gather.18
  72.9 38.9 all-gather.20
  113.8 38.0 all-gather.22
  155.2 30.1 reduce-scatter.2
  187.4 16.6 all-gather.16
  206.3 40.2 all-gather.24
  248.7 38.9 all-gather.26
  289.8 38.0 all-gather.28
  331.2 30.1 reduce-scatter.4
where the time goes:
time: 371 us; the launch traced here: 370 us
  waiting for transfers between devices  290 us (78%)
  blocking collectives  25.3 us (7%)
  matrix products  23.4 us (6%)
  between operations  13.7 us (4%)
  other arithmetic  7.31 us (2%)
  starting transfers between devices  5.32 us (1%)
  local copies, waits for them, and re-layouts  5.19 us (1%)
    all_gather x2, waiting for transfers between devices, shards(): lax.all_gather(w_value[layer], 'sp', axis=0, tiled=True)  81.7 us
    all_gather x2, waiting for transfers between devices, shards(): lax.all_gather(w_gate[layer], 'sp', axis=0, tiled=True)  78.2 us
    reduce_scatter x2, waiting for transfers between devices, shards(): branch = lax.psum_scatter(terms, 'tp', scatter_dimension=1, tiled=True)  60.6 us
    all_gather x2, waiting for transfers between devices, shards(): out_whole = lax.all_gather(w_out[layer], 'sp', axis=1, tiled=True)  32.5 us
    all_gather x2, waiting for transfers between devices, shards(): whole = lax.all_gather(x, 'tp', axis=1, tiled=True).astype(jnp.float32)  30.3 us
    psum x2, blocking collectives, shards(): lax.psum(jnp.sum(centred * centred, axis=1, keepdims=True), 'tp') / C  14 us
    psum x2, blocking collectives, shards(): mean = lax.psum(jnp.sum(conv, axis=1, keepdims=True), 'tp') / C  11.3 us
    conv_general_dilated x2, matrix products, shards(): lax.conv_general_dilated(padded[None], conv_taps[layer][:, None, :], (1,)...  9.67 us
  transfers between devices with their start and end apart: 12, of which 12 were waited for; matrix products, arithmetic and copies ran while one was open for 7% of the time, Pallas kernels for 0%

commit v1 on v0

--- a/solution.py
+++ b/solution.py
@@ -19,7 +19,7 @@
     local_ch = w_value.shape[2]
     taps = conv_taps.shape[1]
     for layer in range(LAYERS):
-        whole = lax.all_gather(x, "tp", axis=1, tiled=True).astype(jnp.float32)
+        whole = jnp.concatenate(jax.lax.all_gather(x, "tp"), 1).astype(jnp.float32)
         normed = (
             whole
             * lax.rsqrt(jnp.mean(whole * whole, axis=1, keepdims=True) + 1e-06)

time: 371 us -> 371 us (level)
  waiting for transfers between devices: 290 us -> 283 us
  local copies, waits for them, and re-layouts: 5.19 us -> 9.19 us
  other arithmetic: 7.31 us -> 11.1 us
    all_gather x2, waiting for transfers between devices: 81.7 us -> 73.8 us  [shards(): lax.all_gather(w_value[layer], 'sp', axis=0, tiled=True)]
    convert_element_type x0 -> x4, other arithmetic: none -> 6.38 us  [the longest x2 5.69 us: shards(): whole = jnp.concatenate(jax.lax.all_gather(x, 'tp'), 1).astype(jnp.float32)]
    convert_element_type x0 -> x2, local copies, waits for them, and re-layouts: none -> 4.01 us  [shards(): whole = jnp.concatenate(jax.lax.all_gather(x, 'tp'), 1).astype(jnp.float32)]
  transfers between devices with their start and end apart: 12 -> 12, of which waited for: 12 -> 12; matrix products, arithmetic and copies ran while one was open for 7% -> 9% of each run, Pallas kernels for 0% -> 0%
where the time goes in v1:
time: 371 us; the launch traced here: 370 us
  waiting for transfers between devices  283 us (76%)
  blocking collectives  25.3 us (7%)
  matrix products  22.7 us (6%)
  between operations  13.7 us (4%)
  other arithmetic  11.1 us (3%)
  local copies, waits for them, and re-layouts  9.19 us (2%)
  starting transfers between devices  5.32 us (1%)
    all_gather x2, waiting for transfers between devices, shards(): lax.all_gather(w_gate[layer], 'sp', axis=0, tiled=True)  78.9 us
    all_gather x2, waiting for transfers between devices, shards(): lax.all_gather(w_value[layer], 'sp', axis=0, tiled=True)  73.8 us
    reduce_scatter x2, waiting for transfers between devices, shards(): branch = lax.psum_scatter(terms, 'tp', scatter_dimension=1, tiled=True)  60.6 us
    all_gather x2, waiting for transfers between devices, shards(): out_whole = lax.all_gather(w_out[layer], 'sp', axis=1, tiled=True)  32.5 us
    all_gather x2, waiting for transfers between devices, shards(): whole = jnp.concatenate(jax.lax.all_gather(x, 'tp'), 1).astype(jnp.float32)  30.3 us
    psum x2, blocking collectives, shards(): lax.psum(jnp.sum(centred * centred, axis=1, keepdims=True), 'tp') / C  14 us
    psum x2, blocking collectives, shards(): mean = lax.psum(jnp.sum(conv, axis=1, keepdims=True), 'tp') / C  11.3 us
    conv_general_dilated x2, matrix products, shards(): lax.conv_general_dilated(padded[None], conv_taps[layer][:, None, :], (1,)...  9.67 us
  transfers between devices with their start and end apart: 12, of which 12 were waited for; matrix products, arithmetic and copies ran while one was open for 9% of the time, Pallas kernels for 0%

profile of v1, /device:TPU:0, one launch (start us, length us, event | category | flops | bytes accessed | tf_op | source)
XLA Modules:
  0.0 370.0 jit_solution(12283603965417174620)
XLA Ops:
  7.3 1.7 fusion.41
  12.7 15.7 %all-gather.17.cloned.1.call-done = bf16[1024,512]{1,0:T(8,128)(2,1)} async-done(((bf16[256,512]{1,0:T(8,128)(2,1)}), bf16[1024,512]{1,0:T(8,128)(2,1)}) %all-gather.17.cloned.1.call-update) | async-done | bytes 1048592 | tf_op jit(solution)/shard_map/all_gather | solution.py:22
  28.3 2.8 convert_bitcast_fusion
  31.2 2.0 copy.17
  33.9 36.9 %all-gather.19.cloned.1.call-done = bf16[1,2048,256]{2,1,0:T(8,128)(2,1)} async-done(((bf16[1,256,256]{2,1,0:T(8,128)(2,1)}), bf16[1,2048,256]{2,1,0:T(8,128)(2,1)}) %all-gather.19.cloned.1.call-update) | async-done | bytes 1048592 | tf_op jit(solution)/shard_map/all_gather | solution.py:29
  70.8 1.7 fusion.23
  72.5 39.5 %all-gather.21.cloned.1.call-done = bf16[1,2048,256]{2,1,0:T(8,128)(2,1)} async-done(((bf16[1,256,256]{2,1,0:T(8,128)(2,1)}), bf16[1,2048,256]{2,1,0:T(8,128)(2,1)}) %all-gather.21.cloned.1.call-update) | async-done | bytes 1048592 | tf_op jit(solution)/shard_map/all_gather | solution.py:30
  111.9 1.7 fusion.13
  113.7 2.5 collective-permute-start
  116.2 1.9 collective-permute-done
  118.1 4.8 %fusion.45 = (f32[256]{0:T(256)S(1)}, f32[1,256,256]{2,0,1:T(1,128)S(1)}) fusion(f32[1,128,256]{2,1,0:T(8,128)S(1)} %get-tuple-element.6, bf16[1,383,256]{2,1,0:T(8,128)(2,1)S(1)} %maximum_bitcast_fusion), kind=kOutput, calls=%fused_computation.71 | convolution fusion | flops 100728576 | bytes 590336 | tf_op jit(solution)/shard_map/conv_general_dilated | solution.py:37
  123.0 5.7 %psum.28 = f32[256,1]{0,1:T(1,128)S(1)} all-reduce(f32[256,1]{0,1:T(1,128)S(1)} %bitcast.98), channel_id=1, replica_groups=mesh['sp'=8,'tp'=4] {'tp'}, use_global_device_ids=true, to_apply=%region_2.0 | all-reduce | flops 256 | bytes 2048 | tf_op jit(solution)/shard_map/psum | solution.py:46
  128.8 7.0 %psum.29 = f32[256,1]{0,1:T(1,128)S(1)} all-reduce(f32[256,1]{0,1:T(1,128)S(1)} %bitcast.94), channel_id=1, replica_groups=mesh['sp'=8,'tp'=4] {'tp'}, use_global_device_ids=true, to_apply=%region_4.0 | all-reduce | flops 256 | bytes 2048 | tf_op jit(solution)/shard_map/psum | solution.py:48
  135.8 16.2 %all-gather.23.cloned.1.call-done = bf16[1,256,2048]{2,1,0:T(8,128)(2,1)} async-done(((bf16[1,256,256]{2,1,0:T(8,128)(2,1)}), bf16[1,256,2048]{2,1,0:T(8,128)(2,1)}) %all-gather.23.cloned.1.call-update) | async-done | bytes 1048592 | tf_op jit(solution)/shard_map/all_gather | solution.py:52
  152.0 3.1 fusion.20
  155.2 30.3 %reduce-scatter.3.cloned.1.call-done = f32[256,512]{1,0:T(8,128)} async-done(((f32[256,2048]{1,0:T(8,128)}), f32[256,512]{1,0:T(8,128)}) %reduce-scatter.3.cloned.1.call-update) | async-done | bytes 524304 | tf_op jit(solution)/shard_map/reduce_scatter | solution.py:54
  185.4 1.8 add_convert_fusion.1
  189.6 14.6 %all-gather.25.cloned.1.call-done = bf16[1024,512]{1,0:T(8,128)(2,1)} async-done(((bf16[256,512]{1,0:T(8,128)(2,1)}), bf16[1024,512]{1,0:T(8,128)(2,1)}) %all-gather.25.cloned.1.call-update) | async-done | bytes 1048592 | tf_op jit(solution)/shard_map/all_gather | solution.py:22
  204.1 2.8 bitcast_convert_fusion
  207.0 2.0 copy.20
  209.7 36.9 %all-gather.27.cloned.1.call-done = bf16[1,2048,256]{2,1,0:T(8,128)(2,1)} async-done(((bf16[1,256,256]{2,1,0:T(8,128)(2,1)}), bf16[1,2048,256]{2,1,0:T(8,128)(2,1)}) %all-gather.27.cloned.1.call-update) | async-done | bytes 1048592 | tf_op jit(solution)/shard_map/all_gather | solution.py:29
  248.3 39.4 %all-gather.29.cloned.1.call-done = bf16[1,2048,256]{2,1,0:T(8,128)(2,1)} async-done(((bf16[1,256,256]{2,1,0:T(8,128)(2,1)}), bf16[1,2048,256]{2,1,0:T(8,128)(2,1)}) %all-gather.29.cloned.1.call-update) | async-done | bytes 1048592 | tf_op jit(solution)/shard_map/all_gather | solution.py:30
  287.7 1.7 fusion.14
  289.5 2.5 collective-permute-start.1
  291.9 1.9 collective-permute-done.1
  293.9 4.8 %fusion.46 = (f32[256]{0:T(256)S(1)}, f32[1,256,256]{2,0,1:T(1,128)S(1)}) fusion(f32[1,128,256]{2,1,0:T(8,128)S(1)} %get-tuple-element.5, bf16[1,383,256]{2,1,0:T(8,128)(2,1)S(1)} %maximum_bitcast_fusion.1), kind=kOutput, calls=%fused_computation.72 | convolution fusion | flops 100728576 | bytes 590336 | tf_op jit(solution)/shard_map/conv_general_dilated | solution.py:37
  298.7 5.7 %psum.30 = f32[256,1]{0,1:T(1,128)S(1)} all-reduce(f32[256,1]{0,1:T(1,128)S(1)} %bitcast.99), channel_id=1, replica_groups=mesh['sp'=8,'tp'=4] {'tp'}, use_global_device_ids=true, to_apply=%region_8.9 | all-reduce | flops 256 | bytes 2048 | tf_op jit(solution)/shard_map/psum | solution.py:46
  304.6 7.0 %psum.31 = f32[256,1]{0,1:T(1,128)S(1)} all-reduce(f32[256,1]{0,1:T(1,128)S(1)} %bitcast.95), channel_id=1, replica_groups=mesh['sp'=8,'tp'=4] {'tp'}, use_global_device_ids=true, to_apply=%region_10.11 | all-reduce | flops 256 | bytes 2048 | tf_op jit(solution)/shard_map/psum | solution.py:48
  311.6 16.3 %all-gather.31.cloned.1.call-done = bf16[1,256,2048]{2,1,0:T(8,128)(2,1)} async-done(((bf16[1,256,256]{2,1,0:T(8,128)(2,1)}), bf16[1,256,2048]{2,1,0:T(8,128)(2,1)}) %all-gather.31.cloned.1.call-update) | async-done | bytes 1048592 | tf_op jit(solution)/shard_map/all_gather | solution.py:52
  327.9 3.1 fusion.15
  331.0 30.3 %reduce-scatter.5.cloned.1.call-done = f32[256,512]{1,0:T(8,128)} async-done(((f32[256,2048]{1,0:T(8,128)}), f32[256,512]{1,0:T(8,128)}) %reduce-scatter.5.cloned.1.call-update) | async-done | bytes 524304 | tf_op jit(solution)/shard_map/reduce_scatter | solution.py:54
  361.4 1.8 add_convert_fusion
  (58 shorter events, 10.2 us)
Async XLA Ops:
  6.5 6.1 %copy-start.5 = (f32[2,2048]{1,0:T(2,128)S(1)}, f32[2,2048]{1,0:T(2,128)}, u32[]{:S(2)}) copy-start(f32[2,2048]{1,0:T(2,128)} %param.8) | copy-start | bytes 49156
  6.5 6.1 %copy-start.4 = (f32[2,128,256]{2,1,0:T(8,128)S(1)}, f32[2,128,256]{2,1,0:T(8,128)}, u32[]{:S(2)}) copy-start(f32[2,128,256]{2,1,0:T(8,128)} %param.11) | copy-start | bytes 786436
  6.5 21.8 %all-gather.17.cloned.1.call-start = ((), (), s32[]{:S(2)}) async-start(), calls=%async_computation.4 | async-start | bytes 1310720 | tf_op jit(solution)/shard_map/all_gather | solution.py:22
  7.3 63.5 %all-gather.19.cloned.1.call-start = ((), (), s32[]{:S(2)}) async-start(), calls=%async_computation.5 | async-start | bytes 1179648 | tf_op jit(solution)/shard_map/all_gather | solution.py:29
  9.0 102.9 %all-gather.21.cloned.1.call-start = ((), (), s32[]{:S(2)}) async-start(), calls=%async_computation.6 | async-start | bytes 1179648 | tf_op jit(solution)/shard_map/all_gather | solution.py:30
  10.8 141.2 %all-gather.23.cloned.1.call-start = ((), (), s32[]{:S(2)}) async-start(), calls=%async_computation.7 | async-start | bytes 1179648 | tf_op jit(solution)/shard_map/all_gather | solution.py:52
  12.5 172.9 %reduce-scatter.3.cloned.1.call-start = ((), (), s32[]{:S(2)}) async-start(), calls=%async_computation.2 | async-start | bytes 2621440 | tf_op jit(solution)/shard_map/reduce_scatter | solution.py:54
  31.2 2.0 copy-start
  33.9 82.3 %copy-start.6 = (f32[2,256]{1,0:T(2,128)S(1)}, f32[2,256]{1,0:T(2,128)}, u32[]{:S(2)}) copy-start(f32[2,256]{1,0:T(2,128)} %param.12) | copy-start | bytes 6148
  113.7 4.4 %collective-permute-start = (bf16[128,256]{1,0:T(8,128)(2,1)S(1)}, bf16[128,256]{1,0:T(8,128)(2,1)S(1)}, u32[]{:S(2)}, u32[]{:S(2)}) collective-permute-start(bf16[128,256]{1,0:T(8,128)(2,1)S(1)} %slice.64), channel_id=1, source_target_pairs={{0,4},{4,8},{8,12},{12,16},{16,20},{20,24},{24,28},{1,5},{5,9},{9,... | collective-permute-start | bytes 196616 | tf_op jit(solution)/shard_map/ppermute | solution.py:13
  152.0 33.5 %copy-start.3 = (bf16[256,512]{1,0:T(8,128)(2,1)S(1)}, bf16[256,512]{1,0:T(8,128)(2,1)}, u32[]{:S(2)}) copy-start(bf16[256,512]{1,0:T(8,128)(2,1)} %param.7) | copy-start | bytes 786436
  155.1 49.0 %all-gather.25.cloned.1.call-start = ((), (), s32[]{:S(2)}) async-start(), calls=%async_computation.8 | async-start | bytes 1310720 | tf_op jit(solution)/shard_map/all_gather | solution.py:22
  187.3 59.3 %all-gather.27.cloned.1.call-start = ((), (), s32[]{:S(2)}) async-start(), calls=%async_computation.9 | async-start | bytes 1179648 | tf_op jit(solution)/shard_map/all_gather | solution.py:29
  188.0 99.7 %all-gather.29.cloned.1.call-start = ((), (), s32[]{:S(2)}) async-start(), calls=%async_computation.10 | async-start | bytes 1179648 | tf_op jit(solution)/shard_map/all_gather | solution.py:30
  188.8 139.1 %all-gather.31.cloned.1.call-start = ((), (), s32[]{:S(2)}) async-start(), calls=%async_computation.11 | async-start | bytes 1179648 | tf_op jit(solution)/shard_map/all_gather | solution.py:52
  189.5 171.9 %reduce-scatter.5.cloned.1.call-start = ((), (), s32[]{:S(2)}) async-start(), calls=%async_computation.3 | async-start | bytes 2621440 | tf_op jit(solution)/shard_map/reduce_scatter | solution.py:54
  207.0 2.0 copy-start.1
  289.5 4.4 %collective-permute-start.1 = (bf16[128,256]{1,0:T(8,128)(2,1)S(1)}, bf16[128,256]{1,0:T(8,128)(2,1)S(1)}, u32[]{:S(2)}, u32[]{:S(2)}) collective-permute-start(bf16[128,256]{1,0:T(8,128)(2,1)S(1)} %slice.66), channel_id=1, source_target_pairs={{0,4},{4,8},{8,12},{12,16},{16,20},{20,24},{24,28},{1,5},{5,9},{9,... | collective-permute-start | bytes 196616 | tf_op jit(solution)/shard_map/ppermute | solution.py:13
  327.9 33.5 %copy-start.2 = (bf16[256,512]{1,0:T(8,128)(2,1)S(1)}, bf16[256,512]{1,0:T(8,128)(2,1)}, u32[]{:S(2)}) copy-start(bf16[256,512]{1,0:T(8,128)(2,1)} %add_convert_fusion.1) | copy-start | bytes 786436
Sparse Core Ops, SparseCore 0:
  8.9 19.4 all-gather.16
  30.5 40.2 all-gather.18
  72.9 38.9 all-gather.20
  113.8 38.0 all-gather.22
  155.2 30.1 reduce-scatter.2
  187.4 16.6 all-gather.24
  206.3 40.2 all-gather.26
  248.7 38.9 all-gather.28
  289.8 38.0 all-gather.30
  331.2 30.1 reduce-scatter.4
